TPU v7x, 256 devices: a 4x2x16 block of a 4x16x16 slice. The times are simulated.
256 devices in a mesh: grp: 2 (over y), ep: 32 (over z, core), tp: 4 (over x).
Axes of the slice: x: 4, y: 2, z: 16, core: 2. Of those that a mesh axis runs over, the one named last changes fastest.
The devices are a block of a 4x16x16 slice.
Arguments:
- query_plain: bfloat16 [16384, 512], P(('grp', 'ep'), 'tp'), parts along dimension 0, may hold values from -400 to 400
- query_rotary: bfloat16 [16384, 256], P(('grp', 'ep'), 'tp'), parts along dimension 0, may hold values from -6 to 6
- latent_input: bfloat16 [16384, 256], P(('grp', 'ep')), parts along dimension 0, may hold values from -6 to 6
- rotary_key: bfloat16 [16384, 32], P(('grp', 'ep')), parts along dimension 0, may hold values from -6 to 6
- key_weight: bfloat16 [256, 512], P(None, 'tp'), may hold values from -0.375 to 0.375
- value_weight: bfloat16 [256, 512], P(None, 'tp'), may hold values from -0.375 to 0.375
- latent_gain: bfloat16 [256], replicated, may hold values from 0.099609375 to 1.8984375
- head_gain: bfloat16 [512], P('tp'), may hold values from 0.099609375 to 1.8984375
- out_weight: bfloat16 [512, 2048], P('tp'), may hold values from -0.25 to 0.25
- expert_input: bfloat16 [32768, 2048], P(('grp', 'ep', 'tp')), parts along dimension 0, may hold values from -6 to 6
- expert_gain: bfloat16 [2048], replicated, may hold values from 0.099609375 to 1.8984375
- routes: int32 [32768, 2], P(('grp', 'ep', 'tp')), parts along dimension 0, may hold values from 0 to 31, all different within a row; in each aligned block of 128 rows (0 to 127, 128 to 255, ...) at most 9 rows name the same one
- route_weight: float32 [32768, 2], P(('grp', 'ep', 'tp')), parts along dimension 0, may hold values from 0.1 to 1
- gate_weight: bfloat16 [32, 2048, 3584], P('ep', None, 'tp'), may hold values from -0.125 to 0.125
- up_weight: bfloat16 [32, 2048, 3584], P('ep', None, 'tp'), may hold values from -0.125 to 0.125
- down_weight: bfloat16 [32, 3584, 2048], P('ep', 'tp'), may hold values from -0.09375 to 0.09375
Outputs:
- attended: bfloat16 [16384, 2048], P(('grp', 'ep', 'tp')), parts along dimension 0
- expert_out: bfloat16 [32768, 2048], P(('grp', 'ep', 'tp')), parts along dimension 0
There are 2 independent parts, one for each index of `grp`. A program takes and returns all parts, laid end to end along the dimension named above; an argument that names none is the same for every part. Nothing has to cross between parts.
Inputs may be any that keep to these rules, and one draw needn't show every extreme that they name: `routes`: each of the 128 rows of one device names 2 different experts; no expert is named by more than 9 rows of one device, a bound that some block reaches of some device.
All inputs are finite; a program needn't handle non-finite values.
Results may differ from a plain program's by a relative error of at most 0.012.
Values may be sent and summed in bfloat16 or wider, within the bound.
No kernel may reach another device: no remote copies, remote signals or barrier semaphores. Data moves between devices by JAX's collectives and lax.ppermute only.
A program may use at most 128 MiB of HBM per device.

v0:
```python
import jax
import jax.numpy as jnp
from jax import lax
from jax.sharding import Mesh
from jax.sharding import PartitionSpec as P

PLAIN_DIM = 64
ROTARY_DIM = 32
VALUE_DIM = 64
TOP = 2
EP = ("ep_0", "ep_1")
GRP_EP = ("grp", "ep_0", "ep_1")
GRP_EP_TP = ("grp", "ep_0", "ep_1", "tp")
EPSILON = 1e-06
THETA = 10000.0
key_span = 2048


def sent_together(arrays, axis, dim, along):
    ends, at = ([], 0)
    for a in arrays[:-1]:
        at += a.shape[along]
        ends.append(at)
    both = jnp.concatenate(arrays, axis=along)
    return tuple(jnp.split(lax.all_gather(both, axis, axis=dim, tiled=True), ends, axis=along))


def in_blocks(array, dim, size):
    lengths = array.shape
    tiles = array.reshape(*lengths[:dim], size, lengths[dim] // size, *lengths[dim + 1 :])
    return jnp.moveaxis(tiles, dim, 0)


def sum_at_owner(array, axis, dim):
    size = lax.axis_size(axis)
    tiles = lax.all_to_all(in_blocks(array, dim, size), axis, 0, 0, tiled=True)
    return jnp.sum(tiles.astype(jnp.float32), axis=0)


def joined_along(tiles, dim):
    tiles = jnp.moveaxis(tiles, 0, dim)
    lengths = tiles.shape
    return tiles.reshape(*lengths[:dim], lengths[dim] * lengths[dim + 1], *lengths[dim + 2 :])


def moved_by_axis(tiles, axes, sequence):
    lengths = [lax.axis_size(a) for a in axes]
    tiles = tiles.reshape(*lengths, *tiles.shape[1:])
    for k in sequence:
        tiles = lax.all_to_all(tiles, axes[k], split_axis=k, concat_axis=k, tiled=True)
    return tiles.reshape(-1, *tiles.shape[len(axes) :])


def two_step_exchange(array, groups, sequence, split_dim, concat_dim):
    size = lax.axis_size(groups[0]) * lax.axis_size(groups[1])
    tiles = in_blocks(array, split_dim, size)
    return joined_along(moved_by_axis(tiles, groups, sequence), concat_dim)


def normalize(entries, gain):
    wide = entries.astype(jnp.float32)
    factor = lax.rsqrt(jnp.mean(wide * wide, axis=-1, keepdims=True) + EPSILON)
    return wide * factor * gain.astype(jnp.float32)


def rotate(entries, positions):
    half = entries.shape[-1] // 2
    freqs = THETA ** (-jnp.arange(half, dtype=jnp.float32) / half)
    angle = positions.astype(jnp.float32)[:, None, None] * freqs[None, None, :]
    cosine = jnp.cos(angle)
    sine = jnp.sin(angle)
    first = entries[..., :half].astype(jnp.float32)
    second = entries[..., half:].astype(jnp.float32)
    turned = jnp.concatenate(
        [first * cosine - second * sine, first * sine + second * cosine], axis=-1
    )
    return turned.astype(jnp.bfloat16)


def rounded(entries):
    return lax.optimization_barrier(entries.astype(jnp.bfloat16)).astype(jnp.float32)


def attend(
    query_plain,
    query_rotary,
    latent_input,
    rotary_key,
    key_weight,
    value_weight,
    latent_gain,
    head_gain,
    out_weight,
):
    tokens = query_plain.shape[0]
    heads = key_weight.shape[1] // PLAIN_DIM
    offset = lax.axis_index(EP) * tokens
    positions = offset + jnp.arange(tokens, dtype=jnp.int32)
    last_position = offset + tokens - 1
    latent = normalize(latent_input, latent_gain).astype(jnp.bfloat16)
    key_rotated = rotate(rotary_key.reshape(tokens, 1, ROTARY_DIM), positions).reshape(
        tokens, ROTARY_DIM
    )
    query_rotated = rotate(query_rotary.reshape(tokens, heads, ROTARY_DIM), positions)
    queries = query_plain.reshape(tokens, heads, PLAIN_DIM)
    factor = (PLAIN_DIM + ROTARY_DIM) ** (-0.5)

    def reshape_given(piece):
        key_rows, value_rows, rotated_rows = piece
        count = key_rows.shape[0]
        return (
            key_rows.reshape(count, heads, PLAIN_DIM),
            value_rows.reshape(count, heads, VALUE_DIM),
            rotated_rows,
        )

    def add_keys(carry, unpacked, start):
        total, highest = carry
        keys, values, rotated_rows = unpacked
        count = keys.shape[0]
        scores = jnp.einsum("qhd,khd->qhk", queries, keys, preferred_element_type=jnp.float32)
        scores = scores + jnp.einsum(
            "qhr,kr->qhk", query_rotated, rotated_rows, preferred_element_type=jnp.float32
        )
        scores = scores * factor
        key_positions = start + jnp.arange(count, dtype=jnp.int32)
        allowed = (key_positions[None, :] <= positions[:, None])[:, None, :]
        masked = jnp.where(allowed, scores, -1e30)
        newest = jnp.maximum(highest, jnp.max(masked, axis=-1))
        weights = jnp.where(allowed, jnp.exp(masked - newest[..., None]), 0.0).astype(jnp.bfloat16)
        total = total * jnp.exp(highest - newest)[..., None] + jnp.einsum(
            "qhk,khd->qhd", weights, values, preferred_element_type=jnp.float32
        )
        return (total, newest)

    def make_fold(unpack):

        def guarded(carry, piece, start):

            def compute(state):
                return add_keys(state, unpack(piece), start)

            def keep(state):
                return state

            return lax.cond(start > last_position, keep, compute, carry)

        def fold(carry, piece, start):
            count = piece[0].shape[0]

            def step(index, inner):
                begin = index * key_span
                sliced = tuple(
                    (lax.dynamic_slice_in_dim(member, begin, key_span, 0) for member in piece)
                )
                return guarded(inner, sliced, begin)

            return lax.fori_loop(0, count // key_span, step, carry)

        return fold

    initial = (
        jnp.zeros((tokens, heads, VALUE_DIM), jnp.float32),
        jnp.full((tokens, heads), -1e30, jnp.float32),
    )
    own_keys = jnp.dot(latent, key_weight, preferred_element_type=jnp.float32).astype(jnp.bfloat16)
    own_values = jnp.dot(latent, value_weight, preferred_element_type=jnp.float32).astype(
        jnp.bfloat16
    )
    folded = make_fold(reshape_given)(
        initial, sent_together((own_keys, own_values, key_rotated), EP, 0, 1), jnp.int32(0)
    )
    context = folded[0]
    head_output = (
        normalize(context, head_gain.reshape(heads, VALUE_DIM))
        .astype(jnp.bfloat16)
        .reshape(tokens, heads * VALUE_DIM)
    )
    summed = sum_at_owner(
        rounded(jnp.dot(head_output, out_weight, preferred_element_type=jnp.float32)).astype(
            jnp.bfloat16
        ),
        "tp",
        0,
    )
    return summed.astype(jnp.bfloat16)


def experts(expert_input, expert_gain, routes, route_weight, gate_weight, up_weight, down_weight):
    tokens = expert_input.shape[0]
    features = expert_input.shape[1]
    count_ep = lax.axis_size(EP)
    capacity = min(tokens, max(2, (9 * tokens + 4 * count_ep - 1) // (4 * count_ep)))
    normed = normalize(expert_input, expert_gain).astype(jnp.bfloat16)
    chosen = routes.reshape(-1)
    onehot = (chosen[:, None] == jnp.arange(count_ep, dtype=jnp.int32)[None, :]).astype(jnp.int32)
    ranks = jnp.sum(jnp.cumsum(onehot, axis=0) * onehot, axis=1) - 1
    destination = chosen * capacity + ranks
    outgoing = (
        jnp.zeros((count_ep * capacity, features), jnp.bfloat16)
        .at[destination]
        .set(jnp.repeat(normed, TOP, axis=0))
    )
    gate_local = gate_weight[0]
    up_local = up_weight[0]
    down_local = down_weight[0]
    arrived = two_step_exchange(outgoing, ("ep_0", "ep_1"), (1, 0), 0, 0)
    piece = lax.all_gather(arrived, "tp", axis=0, tiled=True)
    gate = jnp.dot(piece, gate_local, preferred_element_type=jnp.float32)
    upward = jnp.dot(piece, up_local, preferred_element_type=jnp.float32)
    hidden = (jax.nn.silu(gate) * upward).astype(jnp.bfloat16)
    summed = sum_at_owner(
        rounded(jnp.dot(hidden, down_local, preferred_element_type=jnp.float32)).astype(
            jnp.bfloat16
        ),
        "tp",
        0,
    ).astype(jnp.bfloat16)
    returned = lax.all_to_all(summed, EP, split_axis=0, concat_axis=0, tiled=True)
    picked = returned[destination].astype(jnp.float32).reshape(tokens, TOP, features)
    combined = jnp.sum(picked * route_weight[:, :, None], axis=1)
    return combined.astype(jnp.bfloat16)


def body(
    query_plain,
    query_rotary,
    latent_input,
    rotary_key,
    key_weight,
    value_weight,
    latent_gain,
    head_gain,
    out_weight,
    expert_input,
    expert_gain,
    routes,
    route_weight,
    gate_weight,
    up_weight,
    down_weight,
):
    attended = attend(
        query_plain,
        query_rotary,
        latent_input,
        rotary_key,
        key_weight,
        value_weight,
        latent_gain,
        head_gain,
        out_weight,
    )
    expert_out = experts(
        expert_input, expert_gain, routes, route_weight, gate_weight, up_weight, down_weight
    )
    return (attended, expert_out)


def solution(mesh):
    finer = Mesh(
        mesh.devices.reshape(mesh.shape["grp"], 16, 2, mesh.shape["tp"]),
        ("grp", "ep_0", "ep_1", "tp"),
    )
    in_specs = (
        P(GRP_EP, "tp"),
        P(GRP_EP, "tp"),
        P(GRP_EP, None),
        P(GRP_EP, None),
        P(None, "tp"),
        P(None, "tp"),
        P(),
        P("tp"),
        P("tp", None),
        P(GRP_EP_TP, None),
        P(),
        P(GRP_EP_TP, None),
        P(GRP_EP_TP, None),
        P(EP, None, "tp"),
        P(EP, None, "tp"),
        P(EP, "tp", None),
    )
    out_specs = (P(GRP_EP_TP, None), P(GRP_EP_TP, None))
    return jax.shard_map(body, mesh=finer, in_specs=in_specs, out_specs=out_specs, check_vma=False)
```

profile of v0, /device:TPU:33, one launch (start us, length us, event | category | flops | bytes accessed | tf_op | source)
XLA Modules:
  0.0 412.7 jit_solution(7010274078072165320)
XLA Ops:
  10.9 1.2 fusion.19
  12.2 1.2 fusion.21
  14.5 3.2 scatter_custom_fusion
  17.7 1.6 reshape_reshape.6
  20.0 24.7 %all_to_all.32 = bf16[16,2,9,2048]{3,0,2,1:T(8,128)(2,1)S(1)} all-to-all(bf16[16,2,9,2048]{3,0,2,1:T(8,128)(2,1)S(1)} %copy.34), channel_id=1, replica_groups=mesh['grp'=2,'ep_0'=16,'ep_1'=2,'tp'=4] {'ep_1'}, dimensions={1} | all-to-all | bytes 2359296 | tf_op jit(solution)/shard_map/all_to_all | solution.py:50
  44.7 1.2 copy.35
  46.0 61.2 %all_to_all.33 = bf16[16,2,9,2048]{3,1,2,0:T(2,128)(2,1)S(1)} all-to-all(bf16[16,2,9,2048]{3,1,2,0:T(2,128)(2,1)S(1)} %copy.35), channel_id=1, replica_groups=mesh['grp'=2,'ep_0'=16,'ep_1'=2,'tp'=4] {'ep_0'}, dimensions={0} | all-to-all | bytes 2359296 | tf_op jit(solution)/shard_map/all_to_all | solution.py:50
  107.8 1.4 reshape_reshape.7
  111.2 53.7 %all-gather.5.cloned.1.call-done = bf16[1152,2048]{1,0:T(8,128)(2,1)} async-done(((bf16[288,2048]{1,0:T(8,128)(2,1)}), bf16[1152,2048]{1,0:T(8,128)(2,1)}) %all-gather.5.cloned.1.call-update) | async-done | bytes 4718608 | tf_op jit(solution)/shard_map/all_gather | solution.py:208
  164.9 8.1 %fusion.14 = f32[1152,896]{1,0:T(8,128)S(1)} fusion(bf16[1152,2048]{1,0:T(8,128)(2,1)} %all-gather.5.cloned.1.call-done, bf16[1,2048,896]{2,1,0:T(8,128)(2,1)} %param.33), kind=kOutput, calls=%fused_computation.25 | convolution fusion | flops 4227858432 | bytes 12517376 | tf_op jit(solution)/shard_map/dot_general | solution.py:209
  173.0 5.3 %fusion.16 = bf16[1152,896]{1,0:T(8,128)(2,1)S(1)} fusion(bf16[1152,2048]{1,0:T(8,128)(2,1)S(1)} %copy-done.6, bf16[1,2048,896]{2,1,0:T(8,128)(2,1)S(1)} %copy-done.7, f32[1152,896]{1,0:T(8,128)S(1)} %fusion.14), kind=kOutput, calls=%fused_computation.27 | convolution fusion | flops 4234051584 | bytes 14581760 | tf_op jit(solution)/shard_map/dot_general | solution.py:210
  178.4 6.8 %convolution_convert_fusion = bf16[1152,2048]{1,0:T(8,128)(2,1)} fusion(bf16[1152,896]{1,0:T(8,128)(2,1)S(1)} %fusion.16, bf16[1,896,2048]{2,1,0:T(8,128)(2,1)S(1)} %copy-done.8), kind=kOutput, calls=%fused_computation.21 | convolution fusion | flops 4230217728 | bytes 10452992 | tf_op jit(solution)/shard_map/dot_general | solution.py:213
  185.1 5.1 %all-to-all-start.3 = ((bf16[4,288,2048]{2,1,0:T(8,128)(2,1)}), bf16[4,288,2048]{2,1,0:T(8,128)(2,1)}, u32[]{:S(2)}, u32[]{:S(2)}) async-start(bf16[4,288,2048]{2,1,0:T(8,128)(2,1)} %bitcast.70), calls=%async_computation.3 | async-start | bytes 9437184 | tf_op jit(solution)/shard_map/all_to_all | solution.py:36
  190.7 57.7 %all-gather.3.cloned.1.call-done = bf16[8192,288]{0,1:T(8,128)(2,1)} async-done(((bf16[256,288]{0,1:T(8,128)(2,1)}), bf16[8192,288]{0,1:T(8,128)(2,1)}) %all-gather.3.cloned.1.call-update) | async-done | bytes 4718608 | tf_op jit(solution)/shard_map/all_gather | solution.py:25
  248.4 1.1 split.13
  249.5 3.9 fusion.47
  253.4 4.5 %while.16 = (s32[]{:T(128)}, f32[256,2,64]{0,2,1:T(8,128)S(1)}, f32[256,2]{0,1:T(2,128)S(1)}, s32[]{:T(128)}, bf16[8192,128]{0,1:T(8,128)(2,1)}, /*index=5*/bf16...) while((s32[]{:T(128)}, f32[256,2,64]{0,2,1:T(8,128)S(1)}, ...), condition=%wide.region_5.6_spmd.clone, body=%wide.region_1.5_spmd.clone.sunk | while | flops 343476992 | bytes 22022456 | solution.py:158
  253.4 4.3 %conditional.3 = ((f32[256,2,64]{0,2,1:T(8,128)S(1)}, f32[256,2]{0,1:T(2,128)S(1)})) conditional(s32[]{:T(128)} %convert_element_type.210, (s32[]{:T(128)}, s32[]{:T(128)}, bf16[8192,128]{0,1:T(8,128)(2,1)}, bf16[256,2,64]{0,2,1:T(8,128)(2,1)S(1)}, bf16[8192,32]{0,1:T(8,128)(2,1)S(1)}, /*index=5*/bf16[256,2,32]{0,2,1:T(8,128)(2,1)S(1)}, ...), branch_computations={%region_2.3_spmd, %region_4.4_spmd} | conditional | flops 343476992 | bytes 22021194 | solution.py:146
  253.5 1.1 constant_dynamic-slice_fusion
  255.8 1.1 fusion.46
  258.1 1.4 convolution_convert_fusion.1
  259.5 3.7 all-to-all-start
  263.2 3.3 reduce_sum.74
  266.6 1.6 all_to_all.24
  268.2 9.7 %all-to-all-done = bf16[4,64,2048]{2,1,0:T(8,128)(2,1)S(1)} async-done(((bf16[4,64,2048]{2,1,0:T(8,128)(2,1)}), bf16[4,64,2048]{2,1,0:T(8,128)(2,1)S(1)}, u32[]{:S(2)}, u32[]{:S(2)}) %all-to-all-start) | async-done | bytes 1048608 | tf_op jit(solution)/shard_map/all_to_all | solution.py:36
  277.9 18.7 %all-to-all-start.4 = ((bf16[32,9,2048]{2,1,0:T(8,128)(2,1)}), bf16[32,9,2048]{2,1,0:T(8,128)(2,1)}, u32[]{:S(2)}, u32[]{:S(2)}) async-start(bf16[32,9,2048]{2,1,0:T(8,128)(2,1)} %all_to_all.24), calls=%async_computation.4 | async-start | bytes 4194304 | tf_op jit(solution)/shard_map/all_to_all | solution.py:219
  296.7 0.9 reduce_sum.71
  297.7 97.7 %all-to-all-done.4 = bf16[32,9,2048]{2,1,0:T(8,128)(2,1)} async-done(((bf16[32,9,2048]{2,1,0:T(8,128)(2,1)}), bf16[32,9,2048]{2,1,0:T(8,128)(2,1)}, u32[]{:S(2)}, u32[]{:S(2)}) %all-to-all-start.4) | async-done | bytes 1179680 | tf_op jit(solution)/shard_map/all_to_all | solution.py:219
  395.3 1.8 all_to_all.26
  397.2 2.3 gather_fusion
  399.5 2.4 reshape.297
  401.9 3.9 multiply_reduce_fusion
  (85 shorter events, 10.8 us)
Async XLA Ops:
  7.2 250.9 %copy-start = (bf16[128,2048]{1,0:T(8,128)(2,1)S(1)}, bf16[128,2048]{1,0:T(8,128)(2,1)}, u32[]{:S(2)}) copy-start(bf16[128,2048]{1,0:T(8,128)(2,1)} %param.28) | copy-start | bytes 1572868
  7.2 157.7 %all-gather.5.cloned.1.call-start = ((), (), s32[]{:S(2)}) async-start(), calls=%async_computation.6 | async-start | bytes 5898240 | tf_op jit(solution)/shard_map/all_gather | solution.py:208
  107.1 2.4 copy-start.11
  107.1 2.4 copy-start.1
  107.1 2.6 copy-start.4
  107.1 2.7 copy-start.9
  107.2 3.0 copy-start.10
  109.3 139.1 %all-gather.3.cloned.1.call-start = ((), (), s32[]{:S(2)}) async-start(), calls=%async_computation.5 | async-start | bytes 4866048 | tf_op jit(solution)/shard_map/all_gather | solution.py:25
  164.9 8.1 %copy-start.6 = (bf16[1152,2048]{1,0:T(8,128)(2,1)S(1)}, bf16[1152,2048]{1,0:T(8,128)(2,1)}, u32[]{:S(2)}) copy-start(bf16[1152,2048]{1,0:T(8,128)(2,1)} %all-gather.5.cloned.1.call-done) | copy-start | bytes 14155780
  164.9 8.1 %copy-start.7 = (bf16[1,2048,896]{2,1,0:T(8,128)(2,1)S(1)}, bf16[1,2048,896]{2,1,0:T(8,128)(2,1)}, u32[]{:S(2)}) copy-start(bf16[1,2048,896]{2,1,0:T(8,128)(2,1)} %param.34) | copy-start | bytes 11010052
  173.0 5.3 %copy-start.8 = (bf16[1,896,2048]{2,1,0:T(8,128)(2,1)S(1)}, bf16[1,896,2048]{2,1,0:T(8,128)(2,1)}, u32[]{:S(2)}) copy-start(bf16[1,896,2048]{2,1,0:T(8,128)(2,1)} %param.35) | copy-start | bytes 11010052
  185.1 5.2 %copy-start.2 = (bf16[256,128]{1,0:T(8,128)(2,1)S(1)}, bf16[256,128]{1,0:T(8,128)(2,1)}, u32[]{:S(2)}) copy-start(bf16[256,128]{1,0:T(8,128)(2,1)} %param.20) | copy-start | bytes 196612
  185.1 5.3 %copy-start.12 = (bf16[128]{0:T(256)(128)(2,1)S(1)}, bf16[128]{0:T(256)(128)(2,1)}, u32[]{:S(2)}) copy-start(bf16[128]{0:T(256)(128)(2,1)} %param.27) | copy-start | bytes 772
  185.1 5.5 %copy-start.3 = (bf16[256,64]{0,1:T(8,128)(2,1)S(1)}, bf16[256,64]{0,1:T(8,128)(2,1)}, u32[]{:S(2)}) copy-start(bf16[256,64]{0,1:T(8,128)(2,1)} %param.21) | copy-start | bytes 98308
  185.1 74.4 %all-to-all-start.3 = ((bf16[4,288,2048]{2,1,0:T(8,128)(2,1)}), bf16[4,288,2048]{2,1,0:T(8,128)(2,1)}, u32[]{:S(2)}, u32[]{:S(2)}) async-start(bf16[4,288,2048]{2,1,0:T(8,128)(2,1)} %bitcast.70), calls=%async_computation.3 | async-start | bytes 9437184 | tf_op jit(solution)/shard_map/all_to_all | solution.py:36
  259.5 18.3 %all-to-all-start = ((bf16[4,64,2048]{2,1,0:T(8,128)(2,1)}), bf16[4,64,2048]{2,1,0:T(8,128)(2,1)S(1)}, u32[]{:S(2)}, u32[]{:S(2)}) async-start(bf16[4,64,2048]{2,1,0:T(8,128)(2,1)} %bitcast.12), calls=%async_computation | async-start | bytes 2097152 | tf_op jit(solution)/shard_map/all_to_all | solution.py:36
  266.6 30.1 %copy-start.5 = (f32[128,2]{0,1:T(2,128)S(1)}, f32[128,2]{0,1:T(2,128)}, u32[]{:S(2)}) copy-start(f32[128,2]{0,1:T(2,128)} %param.32) | copy-start | bytes 3076
  277.9 117.5 %all-to-all-start.4 = ((bf16[32,9,2048]{2,1,0:T(8,128)(2,1)}), bf16[32,9,2048]{2,1,0:T(8,128)(2,1)}, u32[]{:S(2)}, u32[]{:S(2)}) async-start(bf16[32,9,2048]{2,1,0:T(8,128)(2,1)} %all_to_all.24), calls=%async_computation.4 | async-start | bytes 4194304 | tf_op jit(solution)/shard_map/all_to_all | solution.py:219
Sparse Core Ops, SparseCore 0:
  109.4 55.4 all-gather.4
  167.2 81.1 all-gather.2
where the time goes:
time: 414 us; the launch traced here: 413 us
  waiting for transfers between devices  219 us (53%)
  blocking collectives  85.9 us (21%)
  starting transfers between devices  27.9 us (7%)
  local copies, waits for them, and re-layouts  25.9 us (6%)
  matrix products  24.8 us (6%)
  other arithmetic  14.5 us (4%)
  between operations  14.5 us (4%)
    all_to_all x1, waiting for transfers between devices, experts(): lax.all_to_all(summed, EP, split_axis=0, concat_axis=0, tiled=True)  97.7 us
    all_to_all x2, blocking collectives, moved_by_axis(): lax.all_to_all(tiles, axes[k], split_axis=k, concat_axis=k, tiled=True)  85.9 us
    all_gather x1, waiting for transfers between devices, sent_together(): lax.all_gather(both, axis, axis=dim, tiled=True)  57.7 us
    all_gather x1, waiting for transfers between devices, experts(): piece = lax.all_gather(arrived, 'tp', axis=0, tiled=True)  53.7 us
    all_to_all x1, starting transfers between devices, experts(): lax.all_to_all(summed, EP, split_axis=0, concat_axis=0, tiled=True)  18.7 us
    all_to_all x2, waiting for transfers between devices, sum_at_owner(): tiles = lax.all_to_all(in_blocks(array, dim, size), axis, 0, 0, tiled=True)  9.7 us
    all_to_all x2, starting transfers between devices, sum_at_owner(): tiles = lax.all_to_all(in_blocks(array, dim, size), axis, 0, 0, tiled=True)  8.82 us
  transfers between devices with their start and end apart: 5, of which 4 were waited for; matrix products, arithmetic and copies ran while one was open for 9% of the time, Pallas kernels for 0%

commit v1 on v0

--- a/solution.py
+++ b/solution.py
@@ -205,7 +205,12 @@
     up_local = up_weight[0]
     down_local = down_weight[0]
     arrived = two_step_exchange(outgoing, ("ep_0", "ep_1"), (1, 0), 0, 0)
-    piece = lax.all_gather(arrived, "tp", axis=0, tiled=True)
+    piece = jnp.concatenate(
+        lax.all_to_all(
+            jnp.stack([arrived] * lax.axis_size("tp"), axis=0), "tp", split_axis=0, concat_axis=0
+        ),
+        axis=0,
+    )
     gate = jnp.dot(piece, gate_local, preferred_element_type=jnp.float32)
     upward = jnp.dot(piece, up_local, preferred_element_type=jnp.float32)
     hidden = (jax.nn.silu(gate) * upward).astype(jnp.bfloat16)

time: 414 us -> 395 us (0.954)
  waiting for transfers between devices: 219 us -> 193 us
  starting transfers between devices: 27.9 us -> 42.9 us
  blocking collectives: 85.9 us -> 77.6 us
  local copies, waits for them, and re-layouts: 25.9 us -> 30.2 us
    all_to_all x2 -> x1, blocking collectives: 85.9 us -> 24.9 us  [moved_by_axis(): lax.all_to_all(tiles, axes[k], split_axis=k, concat_axis=k, tiled=True)]
    all_gather x1, waiting for transfers between devices: 57.7 us -> 0.02 us  [sent_together(): lax.all_gather(both, axis, axis=dim, tiled=True)]
    all_to_all x0 -> x1, waiting for transfers between devices: none -> 54.4 us  [moved_by_axis(): lax.all_to_all(tiles, axes[k], split_axis=k, concat_axis=k, tiled=True)]
    all_gather x1 -> x0, waiting for transfers between devices: 53.7 us -> none  [experts(): piece = lax.all_gather(arrived, 'tp', axis=0, tiled=True)]
    all_to_all x0 -> x1, blocking collectives: none -> 52.8 us  [experts(): lax.all_to_all(jnp.stack([arrived] * lax.axis_size('tp'), axis=0), 'tp',...]
    all_to_all x2, waiting for transfers between devices: 9.7 us -> 40.5 us  [sum_at_owner(): tiles = lax.all_to_all(in_blocks(array, dim, size), axis, 0, 0, tiled=True)]
    all_to_all x1, starting transfers between devices: 18.7 us -> 29.1 us  [experts(): lax.all_to_all(summed, EP, split_axis=0, concat_axis=0, tiled=True)]
    all_to_all x0 -> x1, starting transfers between devices: none -> 4.77 us  [moved_by_axis(): lax.all_to_all(tiles, axes[k], split_axis=k, concat_axis=k, tiled=True)]
  transfers between devices with their start and end apart: 5 -> 5, of which waited for: 4 -> 4; matrix products, arithmetic and copies ran while one was open for 9% -> 10% of each run, Pallas kernels for 0% -> 0%
where the time goes in v1:
time: 395 us; the launch traced here: 394 us
  waiting for transfers between devices  193 us (49%)
  blocking collectives  77.6 us (20%)
  starting transfers between devices  42.9 us (11%)
  local copies, waits for them, and re-layouts  30.2 us (8%)
  matrix products  21.8 us (6%)
  other arithmetic  14.5 us (4%)
  between operations  14.5 us (4%)
    all_to_all x1, waiting for transfers between devices, experts(): lax.all_to_all(summed, EP, split_axis=0, concat_axis=0, tiled=True)  97.7 us
    all_to_all x1, waiting for transfers between devices, moved_by_axis(): lax.all_to_all(tiles, axes[k], split_axis=k, concat_axis=k, tiled=True)  54.4 us
    all_to_all x1, blocking collectives, experts(): lax.all_to_all(jnp.stack([arrived] * lax.axis_size('tp'), axis=0), 'tp',...  52.8 us
    all_to_all x2, waiting for transfers between devices, sum_at_owner(): tiles = lax.all_to_all(in_blocks(array, dim, size), axis, 0, 0, tiled=True)  40.5 us
    all_to_all x1, starting transfers between devices, experts(): lax.all_to_all(summed, EP, split_axis=0, concat_axis=0, tiled=True)  29.1 us
    all_to_all x1, blocking collectives, moved_by_axis(): lax.all_to_all(tiles, axes[k], split_axis=k, concat_axis=k, tiled=True)  24.9 us
    all_to_all x2, starting transfers between devices, sum_at_owner(): tiles = lax.all_to_all(in_blocks(array, dim, size), axis, 0, 0, tiled=True)  8.98 us
  transfers between devices with their start and end apart: 5, of which 4 were waited for; matrix products, arithmetic and copies ran while one was open for 10% of the time, Pallas kernels for 0%

profile of v1, /device:TPU:33, one launch (start us, length us, event | category | flops | bytes accessed | tf_op | source)
XLA Modules:
  0.0 394.4 jit_solution(2050268525110073069)
XLA Ops:
  10.9 1.2 fusion.19
  12.1 1.2 fusion.21
  14.5 3.2 scatter_custom_fusion
  17.7 1.6 reshape_reshape.3
  20.0 24.9 %all_to_all.37 = bf16[16,2,9,2048]{3,0,2,1:T(8,128)(2,1)S(1)} all-to-all(bf16[16,2,9,2048]{3,0,2,1:T(8,128)(2,1)S(1)} %copy.34), channel_id=1, replica_groups=mesh['grp'=2,'ep_0'=16,'ep_1'=2,'tp'=4] {'ep_1'}, dimensions={1} | all-to-all | bytes 2359296 | tf_op jit(solution)/shard_map/all_to_all | solution.py:50
  44.9 2.3 copy.35
  47.1 4.8 %all-to-all-start.2 = ((bf16[16,2,9,2048]{3,1,2,0:T(2,128)(2,1)}), bf16[16,2,9,2048]{3,1,2,0:T(2,128)(2,1)}, u32[]{:S(2)}, u32[]{:S(2)}) async-start(bf16[16,2,9,2048]{3,1,2,0:T(2,128)(2,1)} %copy.35), calls=%async_computation.2 | async-start | bytes 2359296 | tf_op jit(solution)/shard_map/all_to_all | solution.py:50
  53.7 54.4 %all-to-all-done.2 = bf16[16,2,9,2048]{3,1,2,0:T(2,128)(2,1)} async-done(((bf16[16,2,9,2048]{3,1,2,0:T(2,128)(2,1)}), bf16[16,2,9,2048]{3,1,2,0:T(2,128)(2,1)}, u32[]{:S(2)}, u32[]{:S(2)}) %all-to-all-start.2) | async-done | bytes 1179680 | tf_op jit(solution)/shard_map/all_to_all | solution.py:50
  108.1 1.9 copy.36
  110.0 1.4 stack_reshape_reshape.2
  111.4 1.9 stack.3
  113.3 52.8 %all_to_all.38 = bf16[4,288,2048]{2,1,0:T(8,128)(2,1)S(1)} all-to-all(bf16[4,288,2048]{2,1,0:T(8,128)(2,1)S(1)} %stack.3), channel_id=1, replica_groups=mesh['grp'=2,'ep_0'=16,'ep_1'=2,'tp'=4] {'tp'}, dimensions={0} | all-to-all | bytes 9437184 | tf_op jit(solution)/shard_map/all_to_all | solution.py:209
  166.1 5.1 %fusion.14 = f32[1152,896]{1,0:T(8,128)S(1)} fusion(bf16[1152,2048]{1,0:T(8,128)(2,1)S(1)} %bitcast.72, bf16[1,2048,896]{2,1,0:T(8,128)(2,1)S(1)} %copy-done.6), kind=kOutput, calls=%fused_computation.25 | convolution fusion | flops 4227858432 | bytes 12517376 | tf_op jit(solution)/shard_map/dot_general | solution.py:214
  171.2 5.3 %fusion.16 = bf16[1152,896]{1,0:T(8,128)(2,1)S(1)} fusion(bf16[1152,2048]{1,0:T(8,128)(2,1)S(1)} %bitcast.73, bf16[1,2048,896]{2,1,0:T(8,128)(2,1)S(1)} %copy-done.7, f32[1152,896]{1,0:T(8,128)S(1)} %fusion.14), kind=kOutput, calls=%fused_computation.27 | convolution fusion | flops 4234051584 | bytes 14581760 | tf_op jit(solution)/shard_map/dot_general | solution.py:215
  176.6 6.8 %convolution_convert_fusion = bf16[1152,2048]{1,0:T(8,128)(2,1)} fusion(bf16[1152,896]{1,0:T(8,128)(2,1)S(1)} %fusion.16, bf16[1,896,2048]{2,1,0:T(8,128)(2,1)S(1)} %copy-done.8), kind=kOutput, calls=%fused_computation.21 | convolution fusion | flops 4230217728 | bytes 10452992 | tf_op jit(solution)/shard_map/dot_general | solution.py:218
  183.3 5.2 %all-to-all-start.4 = ((bf16[4,288,2048]{2,1,0:T(8,128)(2,1)}), bf16[4,288,2048]{2,1,0:T(8,128)(2,1)}, u32[]{:S(2)}, u32[]{:S(2)}) async-start(bf16[4,288,2048]{2,1,0:T(8,128)(2,1)} %bitcast.71), calls=%async_computation.4 | async-start | bytes 9437184 | tf_op jit(solution)/shard_map/all_to_all | solution.py:36
  190.0 3.9 fusion.47
  193.9 4.5 %while.16 = (s32[]{:T(128)}, f32[256,2,64]{0,2,1:T(8,128)S(1)}, f32[256,2]{0,1:T(2,128)S(1)}, s32[]{:T(128)}, bf16[8192,128]{0,1:T(8,128)(2,1)}, /*index=5*/bf16...) while((s32[]{:T(128)}, f32[256,2,64]{0,2,1:T(8,128)S(1)}, ...), condition=%wide.region_5.6_spmd.clone, body=%wide.region_1.5_spmd.clone.sunk | while | flops 343476992 | bytes 22022456 | solution.py:158
  194.0 4.3 %conditional.3 = ((f32[256,2,64]{0,2,1:T(8,128)S(1)}, f32[256,2]{0,1:T(2,128)S(1)})) conditional(s32[]{:T(128)} %convert_element_type.210, (s32[]{:T(128)}, s32[]{:T(128)}, bf16[8192,128]{0,1:T(8,128)(2,1)}, bf16[256,2,64]{0,2,1:T(8,128)(2,1)S(1)}, bf16[8192,32]{0,1:T(8,128)(2,1)S(1)}, /*index=5*/bf16[256,2,32]{0,2,1:T(8,128)(2,1)S(1)}, ...), branch_computations={%region_2.3_spmd, %region_4.4_spmd} | conditional | flops 343476992 | bytes 22021194 | solution.py:146
  194.0 1.1 constant_dynamic-slice_fusion
  198.6 1.4 convolution_convert_fusion.1
  200.0 36.0 %all-to-all-done.4 = bf16[4,288,2048]{2,1,0:T(8,128)(2,1)} async-done(((bf16[4,288,2048]{2,1,0:T(8,128)(2,1)}), bf16[4,288,2048]{2,1,0:T(8,128)(2,1)}, u32[]{:S(2)}, u32[]{:S(2)}) %all-to-all-start.4) | async-done | bytes 4718624 | tf_op jit(solution)/shard_map/all_to_all | solution.py:36
  236.1 3.8 all-to-all-start
  239.9 3.3 reduce_sum.74
  243.2 1.6 all_to_all.28
  244.8 4.5 %all-to-all-done = bf16[4,64,2048]{2,1,0:T(8,128)(2,1)S(1)} async-done(((bf16[4,64,2048]{2,1,0:T(8,128)(2,1)}), bf16[4,64,2048]{2,1,0:T(8,128)(2,1)S(1)}, u32[]{:S(2)}, u32[]{:S(2)}) %all-to-all-start) | async-done | bytes 1048608 | tf_op jit(solution)/shard_map/all_to_all | solution.py:36
  249.3 29.1 %all-to-all-start.5 = ((bf16[32,9,2048]{2,1,0:T(8,128)(2,1)}), bf16[32,9,2048]{2,1,0:T(8,128)(2,1)}, u32[]{:S(2)}, u32[]{:S(2)}) async-start(bf16[32,9,2048]{2,1,0:T(8,128)(2,1)} %all_to_all.28), calls=%async_computation.5 | async-start | bytes 4194304 | tf_op jit(solution)/shard_map/all_to_all | solution.py:224
  279.4 97.7 %all-to-all-done.5 = bf16[32,9,2048]{2,1,0:T(8,128)(2,1)} async-done(((bf16[32,9,2048]{2,1,0:T(8,128)(2,1)}), bf16[32,9,2048]{2,1,0:T(8,128)(2,1)}, u32[]{:S(2)}, u32[]{:S(2)}) %all-to-all-start.5) | async-done | bytes 1179680 | tf_op jit(solution)/shard_map/all_to_all | solution.py:224
  377.1 1.8 all_to_all.30
  378.9 2.3 gather_fusion
  381.3 2.4 reshape.303
  383.6 3.9 multiply_reduce_fusion
  (85 shorter events, 13.0 us)
Async XLA Ops:
  7.2 191.4 %copy-start = (bf16[128,2048]{1,0:T(8,128)(2,1)S(1)}, bf16[128,2048]{1,0:T(8,128)(2,1)}, u32[]{:S(2)}) copy-start(bf16[128,2048]{1,0:T(8,128)(2,1)} %param.28) | copy-start | bytes 1572868
  20.0 32.0 %copy-start.11 = (bf16[256]{0:T(256)(128)(2,1)S(1)}, bf16[256]{0:T(256)(128)(2,1)}, u32[]{:S(2)}) copy-start(bf16[256]{0:T(256)(128)(2,1)} %param.26) | copy-start | bytes 1540
  20.0 32.1 %copy-start.1 = (bf16[256,256]{1,0:T(8,128)(2,1)S(1)}, bf16[256,256]{1,0:T(8,128)(2,1)}, u32[]{:S(2)}) copy-start(bf16[256,256]{1,0:T(8,128)(2,1)} %param.22) | copy-start | bytes 393220
  20.0 32.2 %copy-start.4 = (bf16[256,32]{0,1:T(8,128)(2,1)S(1)}, bf16[256,32]{0,1:T(8,128)(2,1)}, u32[]{:S(2)}) copy-start(bf16[256,32]{0,1:T(8,128)(2,1)} %param.23) | copy-start | bytes 49156
  20.0 32.4 %copy-start.9 = (bf16[256,128]{1,0:T(8,128)(2,1)S(1)}, bf16[256,128]{1,0:T(8,128)(2,1)}, u32[]{:S(2)}) copy-start(bf16[256,128]{1,0:T(8,128)(2,1)} %param.25) | copy-start | bytes 196612
  20.0 32.6 %copy-start.10 = (bf16[256,128]{1,0:T(8,128)(2,1)S(1)}, bf16[256,128]{1,0:T(8,128)(2,1)}, u32[]{:S(2)}) copy-start(bf16[256,128]{1,0:T(8,128)(2,1)} %param.24) | copy-start | bytes 196612
  47.1 60.9 %all-to-all-start.2 = ((bf16[16,2,9,2048]{3,1,2,0:T(2,128)(2,1)}), bf16[16,2,9,2048]{3,1,2,0:T(2,128)(2,1)}, u32[]{:S(2)}, u32[]{:S(2)}) async-start(bf16[16,2,9,2048]{3,1,2,0:T(2,128)(2,1)} %copy.35), calls=%async_computation.2 | async-start | bytes 2359296 | tf_op jit(solution)/shard_map/all_to_all | solution.py:50
  51.9 137.0 %all-gather.2.cloned.1.call-start = ((), (), s32[]{:S(2)}) async-start(), calls=%async_computation.6 | async-start | bytes 4866048 | tf_op jit(solution)/shard_map/all_gather | solution.py:25
  113.3 52.8 %copy-start.6 = (bf16[1,2048,896]{2,1,0:T(8,128)(2,1)S(1)}, bf16[1,2048,896]{2,1,0:T(8,128)(2,1)}, u32[]{:S(2)}) copy-start(bf16[1,2048,896]{2,1,0:T(8,128)(2,1)} %param.33) | copy-start | bytes 11010052
  166.1 5.1 %copy-start.7 = (bf16[1,2048,896]{2,1,0:T(8,128)(2,1)S(1)}, bf16[1,2048,896]{2,1,0:T(8,128)(2,1)}, u32[]{:S(2)}) copy-start(bf16[1,2048,896]{2,1,0:T(8,128)(2,1)} %param.34) | copy-start | bytes 11010052
  171.2 5.3 %copy-start.8 = (bf16[1,896,2048]{2,1,0:T(8,128)(2,1)S(1)}, bf16[1,896,2048]{2,1,0:T(8,128)(2,1)}, u32[]{:S(2)}) copy-start(bf16[1,896,2048]{2,1,0:T(8,128)(2,1)} %param.35) | copy-start | bytes 11010052
  183.3 5.2 %copy-start.2 = (bf16[256,128]{1,0:T(8,128)(2,1)S(1)}, bf16[256,128]{1,0:T(8,128)(2,1)}, u32[]{:S(2)}) copy-start(bf16[256,128]{1,0:T(8,128)(2,1)} %param.20) | copy-start | bytes 196612
  183.3 5.3 %copy-start.12 = (bf16[128]{0:T(256)(128)(2,1)S(1)}, bf16[128]{0:T(256)(128)(2,1)}, u32[]{:S(2)}) copy-start(bf16[128]{0:T(256)(128)(2,1)} %param.27) | copy-start | bytes 772
  183.3 5.5 %copy-start.3 = (bf16[256,64]{0,1:T(8,128)(2,1)S(1)}, bf16[256,64]{0,1:T(8,128)(2,1)}, u32[]{:S(2)}) copy-start(bf16[256,64]{0,1:T(8,128)(2,1)} %param.21) | copy-start | bytes 98308
  183.3 52.7 %all-to-all-start.4 = ((bf16[4,288,2048]{2,1,0:T(8,128)(2,1)}), bf16[4,288,2048]{2,1,0:T(8,128)(2,1)}, u32[]{:S(2)}, u32[]{:S(2)}) async-start(bf16[4,288,2048]{2,1,0:T(8,128)(2,1)} %bitcast.71), calls=%async_computation.4 | async-start | bytes 9437184 | tf_op jit(solution)/shard_map/all_to_all | solution.py:36
  236.1 13.3 %all-to-all-start = ((bf16[4,64,2048]{2,1,0:T(8,128)(2,1)}), bf16[4,64,2048]{2,1,0:T(8,128)(2,1)S(1)}, u32[]{:S(2)}, u32[]{:S(2)}) async-start(bf16[4,64,2048]{2,1,0:T(8,128)(2,1)} %bitcast.12), calls=%async_computation | async-start | bytes 2097152 | tf_op jit(solution)/shard_map/all_to_all | solution.py:36
  243.2 35.2 %copy-start.5 = (f32[128,2]{0,1:T(2,128)S(1)}, f32[128,2]{0,1:T(2,128)}, u32[]{:S(2)}) copy-start(f32[128,2]{0,1:T(2,128)} %param.32) | copy-start | bytes 3076
  249.3 127.8 %all-to-all-start.5 = ((bf16[32,9,2048]{2,1,0:T(8,128)(2,1)}), bf16[32,9,2048]{2,1,0:T(8,128)(2,1)}, u32[]{:S(2)}, u32[]{:S(2)}) async-start(bf16[32,9,2048]{2,1,0:T(8,128)(2,1)} %all_to_all.28), calls=%async_computation.5 | async-start | bytes 4194304 | tf_op jit(solution)/shard_map/all_to_all | solution.py:224
Sparse Core Ops, SparseCore 0:
  55.1 107.9 all-gather.1
